TPU v7x, 32 devices: a whole 2x2x4 slice. The times are simulated.
32 devices in a mesh: dp: 4 (over y, x), kv: 4 (over z), tp: 2 (over core).
Axes of the slice: x: 2, y: 2, z: 4, core: 2. Of those that a mesh axis runs over, the one named last changes fastest.
Arguments:
- stream: bfloat16 [32, 2048], P('dp', ('kv', 'tp')), parts along dimension 0, may hold values from -40 to 40
- old_state: float32 [32, 8, 64, 128], P(('dp', 'kv'), 'tp'), parts along dimension 0, may hold values from -6 to 6
- decay_amounts: float32 [32, 512], P(('dp', 'kv'), 'tp'), parts along dimension 0, may hold values from 0.003 to 1
- first_gain: float32 [2048], replicated, may hold values from 0.1 to 1.9
- first_gate: bfloat16 [2048, 5632], P(None, ('kv', 'tp')), may hold values from -0.125 to 0.125
- first_up: bfloat16 [2048, 5632], P(None, ('kv', 'tp')), may hold values from -0.125 to 0.125
- first_down: bfloat16 [5632, 2048], P(('kv', 'tp')), may hold values from -0.078125 to 0.078125
- mixer_gain: float32 [2048], P('kv'), may hold values from 0.1 to 1.9
- query_weight: bfloat16 [2048, 512], P('kv', 'tp'), may hold values from -0.125 to 0.125
- key_weight: bfloat16 [2048, 512], P('kv', 'tp'), may hold values from -0.125 to 0.125
- decay_weight: bfloat16 [2048, 512], P('kv', 'tp'), may hold values from -0.5 to 0.5
- value_weight: bfloat16 [2048, 1024], P('kv', 'tp'), may hold values from -0.125 to 0.125
- output_gate_weight: bfloat16 [2048, 1024], P('kv', 'tp'), may hold values from -0.125 to 0.125
- head_gain: float32 [1024], P('tp'), may hold values from 0.1 to 1.9
- output_weight: bfloat16 [1024, 2048], P('tp', 'kv'), may hold values from -0.1875 to 0.1875
- second_gain: float32 [2048], replicated, may hold values from 0.1 to 1.9
- second_gate: bfloat16 [2048, 5632], P(None, ('kv', 'tp')), may hold values from -0.125 to 0.125
- second_up: bfloat16 [2048, 5632], P(None, ('kv', 'tp')), may hold values from -0.125 to 0.125
- second_down: bfloat16 [5632, 2048], P(('kv', 'tp')), may hold values from -0.078125 to 0.078125
Outputs:
- mixed_stream: bfloat16 [32, 2048], P('dp', ('kv', 'tp')), parts along dimension 0
- new_state: float32 [32, 8, 64, 128], P(('dp', 'kv'), 'tp'), parts along dimension 0
There are 4 independent parts, one for each index of `dp`. A program takes and returns all parts, laid end to end along the dimension named above; an argument that names none is the same for every part. Nothing has to cross between parts.
All inputs are finite; a program needn't handle non-finite values.
Results may differ from a plain program's by a relative error of at most 0.007.
Values may be sent and summed in bfloat16 or wider, within the bound.
No kernel may reach another device: no remote copies, remote signals or barrier semaphores. Data moves between devices by JAX's collectives and lax.ppermute only.
A program may use at most 64 MiB of HBM per device.

v0:
```python
import jax
import jax.numpy as jnp
from jax import lax
from jax.sharding import PartitionSpec as P

D = 2048


EPSILON = 1e-06
GATE_SOFTNESS = 16.0


def half_block(stream, norm_gain, w_gate, w_up, w_down):
    wide = lax.all_gather(stream, ("kv", "tp"), axis=1, tiled=True).astype(jnp.float32)
    scaled = (wide * norm_gain).astype(jnp.bfloat16)
    gate_acc = jnp.dot(scaled, w_gate, preferred_element_type=jnp.float32)
    up_acc = jnp.dot(scaled, w_up, preferred_element_type=jnp.float32)
    square_acc = jnp.sum(wide * wide, axis=1)
    row_scale = lax.rsqrt(square_acc / norm_gain.shape[0] + EPSILON)[:, None]
    hidden = (jax.nn.silu(gate_acc * row_scale) * (up_acc * row_scale)).astype(jnp.bfloat16)
    partial_out = jnp.dot(hidden, w_down, preferred_element_type=jnp.float32)
    summed = lax.psum_scatter(partial_out, ("kv", "tp"), scatter_dimension=1, tiled=True)
    return (stream.astype(jnp.float32) + 0.5 * summed).astype(jnp.bfloat16)


def body(
    stream,
    old_state,
    decay_amounts,
    first_gain,
    first_gate,
    first_up,
    first_down,
    mixer_gain,
    query_weight,
    key_weight,
    decay_weight,
    value_weight,
    output_gate_weight,
    head_gain,
    output_weight,
    second_gain,
    second_gate,
    second_up,
    second_down,
):
    middle = half_block(stream, first_gain, first_gate, first_up, first_down)
    paired_cols = lax.all_gather(middle, "tp", axis=1, tiled=True)
    wide_cols = paired_cols.astype(jnp.float32)
    scaled = (wide_cols * mixer_gain).astype(jnp.bfloat16)
    query_part = jnp.dot(scaled, query_weight, preferred_element_type=jnp.float32)
    key_part = jnp.dot(scaled, key_weight, preferred_element_type=jnp.float32)
    decay_part = jnp.dot(scaled, decay_weight, preferred_element_type=jnp.float32)
    value_part = jnp.dot(scaled, value_weight, preferred_element_type=jnp.float32)
    outgate_part = jnp.dot(scaled, output_gate_weight, preferred_element_type=jnp.float32)
    local_rows = old_state.shape[0]
    local_heads = old_state.shape[1]
    key_dim = old_state.shape[2]
    value_dim = old_state.shape[3]
    query_sum, key_sum, decay_sum, value_sum, outgate_sum, own_squares = (
        lax.psum_scatter(query_part, "kv", scatter_dimension=0, tiled=True),
        lax.psum_scatter(key_part, "kv", scatter_dimension=0, tiled=True),
        lax.psum_scatter(decay_part, "kv", scatter_dimension=0, tiled=True),
        lax.psum_scatter(value_part, "kv", scatter_dimension=0, tiled=True),
        lax.psum_scatter(outgate_part, "kv", scatter_dimension=0, tiled=True),
        lax.psum_scatter(
            jnp.sum(wide_cols * wide_cols, axis=1), "kv", scatter_dimension=0, tiled=True
        ),
    )
    row_scale = lax.rsqrt(own_squares / D + EPSILON)[:, None]
    query = (query_sum * row_scale * key_dim ** (-0.5)).reshape(local_rows, local_heads, key_dim)
    keys = (key_sum * row_scale).reshape(local_rows, local_heads, key_dim)
    gate_logits = (decay_sum * row_scale).reshape(local_rows, local_heads, key_dim)
    values = (value_sum * row_scale).reshape(local_rows, local_heads, value_dim)
    decay_logarithm = jax.nn.log_sigmoid(gate_logits) / GATE_SOFTNESS - decay_amounts.reshape(
        local_rows, local_heads, key_dim
    )
    new_state = (
        jnp.exp(decay_logarithm)[..., None] * old_state + keys[..., None] * values[:, :, None, :]
    )
    readout = jnp.einsum("bhk,bhkv->bhv", query, new_state, precision=lax.Precision.HIGHEST)
    normed = readout * lax.rsqrt(jnp.mean(readout * readout, axis=-1, keepdims=True) + EPSILON)
    mixed_heads = (
        normed.reshape(local_rows, local_heads * value_dim)
        * head_gain
        * jax.nn.silu(outgate_sum * row_scale)
    ).astype(jnp.bfloat16)
    projected = jnp.dot(
        lax.all_gather(mixed_heads, "kv", axis=0, tiled=True),
        output_weight,
        preferred_element_type=jnp.float32,
    ).astype(jnp.bfloat16)
    attention_out = lax.psum_scatter(
        lax.optimization_barrier(projected).astype(jnp.float32).astype(jnp.bfloat16),
        "tp",
        scatter_dimension=1,
        tiled=True,
    ).astype(jnp.float32)
    after = (middle.astype(jnp.float32) + attention_out).astype(jnp.bfloat16)
    mixed_stream = half_block(after, second_gain, second_gate, second_up, second_down)
    return (mixed_stream, new_state)


def solution(mesh):
    in_specs = (
        P("dp", ("kv", "tp")),
        P(("dp", "kv"), "tp", None, None),
        P(("dp", "kv"), "tp"),
        P(),
        P(None, ("kv", "tp")),
        P(None, ("kv", "tp")),
        P(("kv", "tp"), None),
        P("kv"),
        P("kv", "tp"),
        P("kv", "tp"),
        P("kv", "tp"),
        P("kv", "tp"),
        P("kv", "tp"),
        P("tp"),
        P("tp", "kv"),
        P(),
        P(None, ("kv", "tp")),
        P(None, ("kv", "tp")),
        P(("kv", "tp"), None),
    )
    out_specs = (P("dp", ("kv", "tp")), P(("dp", "kv"), "tp", None, None))
    return jax.shard_map(body, mesh=mesh, in_specs=in_specs, out_specs=out_specs, check_vma=False)
```

profile of v0, /device:TPU:0, one launch (start us, length us, event | category | flops | bytes accessed | tf_op | source)
XLA Modules:
  0.0 171.4 jit_solution(4641886258188548074)
XLA Ops:
  7.2 16.1 %all_gather.12 = bf16[8,2048]{1,0:T(8,128)(2,1)S(1)} all-gather(bf16[8,256]{1,0:T(8,128)(2,1)} %param.19), channel_id=1, replica_groups=mesh['dp'=4,'kv'=4,'tp'=2] {'kv','tp'}, dimensions={1}, use_global_device_ids=true | all-gather | bytes 36864 | tf_op jit(solution)/shard_map/all_gather | solution.py:14
  23.3 0.1 fusion.7
  23.4 2.7 %convolution_multiply_fusion.3 = f32[8,704]{1,0:T(8,128)S(1)} fusion(bf16[2048,704]{0,1:T(8,128)(2,1)} %param.23, bf16[8,2048]{1,0:T(8,128)(2,1)S(1)} %all_gather.12, f32[2048]{0:T(1024)} %param.22, f32[8]{0:T(128)S(1)} %add_rsqrt_fusion.2), kind=kOutput, calls=%fused_computation.5 | convolution fusion | flops 23123456 | bytes 2947104 | tf_op jit(solution)/shard_map/dot_general | solution.py:16
  26.2 4.2 %fusion.5 = f32[8,2048]{1,0:T(8,128)} fusion(bf16[704,2048]{1,0:T(8,128)(2,1)S(1)} %copy-done, bf16[2048,704]{0,1:T(8,128)(2,1)} %param.24, bf16[8,2048]{1,0:T(8,128)(2,1)S(1)} %all_gather.12, f32[2048]{0:T(1024)S(1)} %copy-done.4, f32[8,704]{1,0:T(8,128)S(1)} %convolution_multiply_fusion.3, f32[8]{0:T(128)S(1)} %add_rsqrt_fusion.2), kind=kOutput, calls=%fused_computation.9 | convolution fusion | flops 46225920 | bytes 5896224 | tf_op jit(solution)/shard_map/dot_general | solution.py:21
  30.5 0.1 reshape.62
  30.5 0.6 dynamic-slice
  31.1 30.9 %reduce-scatter.4.cloned.1.call-done = f32[8,256]{1,0:T(8,128)} async-done(((f32[8,2048]{1,0:T(8,128)}), f32[8,256]{1,0:T(8,128)}) %reduce-scatter.4.cloned.1.call-update) | async-done | bytes 8208 | tf_op jit(solution)/shard_map/reduce_scatter | solution.py:22
  62.0 0.7 add_convert_fusion.2
  62.7 1.8 %all_gather.13 = bf16[8,512]{1,0:T(8,128)(2,1)S(1)} all-gather(bf16[8,256]{1,0:T(8,128)(2,1)S(1)} %add_convert_fusion.2), channel_id=1, replica_groups=mesh['dp'=4,'kv'=4,'tp'=2] {'tp'}, dimensions={1}, use_global_device_ids=true | all-gather | bytes 12288 | tf_op jit(solution)/shard_map/all_gather | solution.py:48
  64.5 0.1 fusion.27
  64.7 1.1 fusion.49
  65.8 1.1 fusion.47
  66.9 1.1 fusion.51
  68.0 0.2 fusion.45
  68.1 1.2 fusion.43
  70.0 16.6 %all-reduce.6 = (f32[8]{0:T(128)S(1)}, f32[8,512]{1,0:T(8,128)S(1)}, f32[8,256]{1,0:T(8,128)S(1)}, f32[8,512]{1,0:T(8,128)S(1)}, f32[8,256]{1,0:T(8,128)S(1)}, /*index=5*/f32[8,256]{1,0:T(8,128)S(1)}) all-reduce(f32[8]{0:T(128)S(1)} %fusion.27, f32[8,512]{1,0:T(8,128)S(1)} %fusion.43, ...), channel_id=4, replica_groups=mesh['dp'=4,'kv'=4,'tp'=2] {'kv'}, use_global_device_ids=true, to_apply=%region_4.5.clone | all-reduce | flops 14344 | bytes 114752
  86.9 0.1 neg.41
  87.0 0.1 mul.191
  87.2 1.1 multiply_add_fusion
  88.4 0.3 fusion.55
  88.7 0.1 multiply_reduce_fusion
  88.8 0.1 fusion.40
  89.0 11.9 %all-gather = bf16[4,2,512]{2,1,0:T(2,128)(2,1)S(1)} all-gather(bf16[1,2,512]{2,1,0:T(2,128)(2,1)S(1)} %fusion.40), channel_id=1, replica_groups=mesh['dp'=4,'kv'=4,'tp'=2] {'kv'}, dimensions={0}, use_global_device_ids=true | all-gather | bytes 10240 | tf_op jit(solution)/shard_map/all_gather | solution.py:89
  100.9 1.8 %convolution_convert_fusion = bf16[8,512]{1,0:T(8,128)(2,1)} fusion(bf16[8,512]{1,0:T(8,128)(2,1)S(1)} %reshape.65, bf16[512,512]{1,0:T(8,128)(2,1)} %param.33), kind=kOutput, calls=%fused_computation.10 | convolution fusion | flops 4198400 | bytes 540672 | tf_op jit(solution)/shard_map/dot_general | solution.py:88
  102.8 6.4 %reduce-scatter.6.cloned.1.call-done = bf16[8,256]{1,0:T(8,128)(2,1)} async-done(((bf16[8,512]{1,0:T(8,128)(2,1)}), bf16[8,256]{1,0:T(8,128)(2,1)}) %reduce-scatter.6.cloned.1.call-update) | async-done | bytes 4112 | tf_op jit(solution)/shard_map/reduce_scatter | solution.py:93
  109.2 0.7 add_convert_fusion.1
  109.8 14.3 %all_gather.15 = bf16[8,2048]{1,0:T(8,128)(2,1)S(1)} all-gather(bf16[8,256]{1,0:T(8,128)(2,1)S(1)} %add_convert_fusion.1), channel_id=1, replica_groups=mesh['dp'=4,'kv'=4,'tp'=2] {'kv','tp'}, dimensions={1}, use_global_device_ids=true | all-gather | bytes 36864 | tf_op jit(solution)/shard_map/all_gather | solution.py:14
  124.2 0.1 fusion.9
  124.3 2.7 %convolution_multiply_fusion.1 = f32[8,704]{1,0:T(8,128)S(1)} fusion(bf16[2048,704]{0,1:T(8,128)(2,1)} %param.35, bf16[8,2048]{1,0:T(8,128)(2,1)S(1)} %all_gather.15, f32[2048]{0:T(1024)S(1)} %copy-done.5, f32[8]{0:T(128)S(1)} %add_rsqrt_fusion.1), kind=kOutput, calls=%fused_computation.2 | convolution fusion | flops 23123456 | bytes 2947104 | tf_op jit(solution)/shard_map/dot_general | solution.py:16
  127.0 5.0 %fusion.4 = f32[8,2048]{1,0:T(8,128)} fusion(bf16[704,2048]{1,0:T(8,128)(2,1)} %param.37, bf16[2048,704]{0,1:T(8,128)(2,1)} %param.36, bf16[8,2048]{1,0:T(8,128)(2,1)S(1)} %all_gather.15, f32[2048]{0:T(1024)S(1)} %copy-done.5, f32[8,704]{1,0:T(8,128)S(1)} %convolution_multiply_fusion.1, f32[8]{0:T(128)S(1)} %add_rsqrt_fusion.1), kind=kOutput, calls=%fused_computation.8 | convolution fusion | flops 46225920 | bytes 5896224 | tf_op jit(solution)/shard_map/dot_general | solution.py:21
  132.0 31.5 %reduce-scatter.8.cloned.1.call-done = f32[8,256]{1,0:T(8,128)} async-done(((f32[8,2048]{1,0:T(8,128)}), f32[8,256]{1,0:T(8,128)}) %reduce-scatter.8.cloned.1.call-update) | async-done | bytes 8208 | tf_op jit(solution)/shard_map/reduce_scatter | solution.py:22
  163.5 1.3 add_convert_fusion
  (37 shorter events, 0.7 us)
Async XLA Ops:
  7.2 19.0 %copy-start = (bf16[704,2048]{1,0:T(8,128)(2,1)S(1)}, bf16[704,2048]{1,0:T(8,128)(2,1)}, u32[]{:S(2)}) copy-start(bf16[704,2048]{1,0:T(8,128)(2,1)} %param.25) | copy-start | bytes 8650756
  7.2 18.9 %copy-start.4 = (f32[2048]{0:T(1024)S(1)}, f32[2048]{0:T(1024)}, u32[]{:S(2)}) copy-start(f32[2048]{0:T(1024)} %param.22) | copy-start | bytes 24580
  7.2 54.8 %reduce-scatter.4.cloned.1.call-start = ((), (), s32[]{:S(2)}) async-start(), calls=%async_computation.3 | async-start | bytes 73728 | tf_op jit(solution)/shard_map/reduce_scatter | solution.py:22
  26.1 4.3 %copy-start.7 = (f32[2,256]{1,0:T(2,128)S(1)}, f32[2,256]{1,0:T(2,128)}, u32[]{:S(2)}) copy-start(f32[2,256]{1,0:T(2,128)} %param.21) | copy-start | bytes 6148
  26.1 4.4 %copy-start.9 = (u32[32]{0:T(128)S(1)}, u32[32]{0:T(128)}, u32[]{:S(2)}) copy-start(u32[32]{0:T(128)} %constant.35) | copy-start | bytes 388
  26.2 35.9 %copy-start.6 = (bf16[8,256]{1,0:T(8,128)(2,1)S(1)}, bf16[8,256]{1,0:T(8,128)(2,1)}, u32[]{:S(2)}) copy-start(bf16[8,256]{1,0:T(8,128)(2,1)} %param.19) | copy-start | bytes 12292
  26.2 38.5 %copy-start.3 = (f32[512]{0:T(512)S(1)}, f32[512]{0:T(512)}, u32[]{:S(2)}) copy-start(f32[512]{0:T(512)} %param.26) | copy-start | bytes 6148
  26.2 41.8 %copy-start.2 = (bf16[512,512]{1,0:T(8,128)(2,1)S(1)}, bf16[512,512]{1,0:T(8,128)(2,1)}, u32[]{:S(2)}) copy-start(bf16[512,512]{1,0:T(8,128)(2,1)} %param.30) | copy-start | bytes 1572868
  30.4 58.5 %copy-start.8 = (f32[512]{0:T(512)S(1)}, f32[512]{0:T(512)}, u32[]{:S(2)}) copy-start(f32[512]{0:T(512)} %param.32) | copy-start | bytes 6148
  30.4 93.9 %copy-start.5 = (f32[2048]{0:T(1024)S(1)}, f32[2048]{0:T(1024)}, u32[]{:S(2)}) copy-start(f32[2048]{0:T(1024)} %param.34) | copy-start | bytes 24580
  30.4 78.8 %reduce-scatter.6.cloned.1.call-start = ((), (), s32[]{:S(2)}) async-start(), calls=%async_computation.4 | async-start | bytes 12288 | tf_op jit(solution)/shard_map/reduce_scatter | solution.py:93
  88.4 43.6 %copy-start.1 = (f32[2,4,64,128]{3,2,1,0:T(8,128)}, f32[2,4,64,128]{3,2,1,0:T(8,128)S(1)}, u32[]{:S(2)}) copy-start(f32[2,4,64,128]{3,2,1,0:T(8,128)S(1)} %multiply_add_fusion) | copy-start | bytes 786436
  102.7 60.8 %reduce-scatter.8.cloned.1.call-start = ((), (), s32[]{:S(2)}) async-start(), calls=%async_computation.5 | async-start | bytes 73728 | tf_op jit(solution)/shard_map/reduce_scatter | solution.py:22
Sparse Core Ops, SparseCore 0:
  30.5 31.4 reduce-scatter.3
  102.9 6.2 reduce-scatter.5
  132.1 31.3 reduce-scatter.7
where the time goes:
time: 172 us; the launch traced here: 171 us
  waiting for transfers between devices  68.8 us (40%)
  blocking collectives  60.8 us (35%)
  matrix products  21.3 us (12%)
  between operations  14.6 us (8%)
  other arithmetic  4.73 us (3%)
    reduce_scatter x2, waiting for transfers between devices, half_block(): lax.psum_scatter(partial_out, ('kv', 'tp'), scatter_dimension=1, tiled=True)  62.4 us
    all_gather x2, blocking collectives, half_block(): lax.all_gather(stream, ('kv', 'tp'), axis=1, tiled=True).astype(jnp.float32)  30.4 us
    unnamed x1, blocking collectives  16.6 us
    all_gather x1, blocking collectives, body(): lax.all_gather(mixed_heads, 'kv', axis=0, tiled=True)  11.9 us
    dot_general x2, matrix products, half_block(): partial_out = jnp.dot(hidden, w_down, preferred_element_type=jnp.float32)  9.16 us
    reduce_scatter x1, waiting for transfers between devices, body(): lax.psum_scatter(lax.optimization_barrier(projected).astype(jnp.float32)....  6.35 us
    dot_general x2, matrix products, half_block(): gate_acc = jnp.dot(scaled, w_gate, preferred_element_type=jnp.float32)  5.33 us
  transfers between devices with their start and end apart: 3, of which 3 were waited for; matrix products, arithmetic and copies ran while one was open for 0% of the time, Pallas kernels for 0%

commit v1 on v0

--- a/solution.py
+++ b/solution.py
@@ -1,13 +1,296 @@
+import functools
+
 import jax
 import jax.numpy as jnp
 from jax import lax
+from jax.experimental import pallas as pl
+from jax.experimental.pallas import tpu as pltpu
 from jax.sharding import PartitionSpec as P
-
-D = 2048
 
 
 EPSILON = 1e-06
 GATE_SOFTNESS = 16.0
+f32 = jnp.float32
+bf16 = jnp.bfloat16
+LANES = 128
+
+
+def shape(dims, dtype=f32):
+    return jax.ShapeDtypeStruct(tuple(dims), dtype)
+
+
+def call(kernel, outs, *args, scratch=(), flops=0, limit=4, moved=None):
+    vmem = pl.BlockSpec(memory_space=pltpu.VMEM)
+    moved = moved or sum(a.size * a.dtype.itemsize for a in args)
+    return pl.pallas_call(
+        kernel,
+        out_shape=outs,
+        in_specs=[vmem] * len(args),
+        out_specs=jax.tree.map(lambda _: vmem, outs),
+        scratch_shapes=list(scratch),
+        cost_estimate=pl.CostEstimate(flops=flops, bytes_accessed=moved, transcendentals=0),
+        compiler_params=pltpu.CompilerParams(vmem_limit_bytes=limit << 20),
+    )(*args)
+
+
+def swap(x, axis, size, shift):
+    return lax.ppermute(x, axis, [(j, j ^ shift) for j in range(size)])
+
+
+def send_kv(blocks, n_kv):
+    got = []
+    for s in range(1, n_kv):
+        got.append(swap(blocks[s - 1], "kv", n_kv, s))
+    return got
+
+
+def silu(x):
+    return x / (1.0 + jnp.exp(-x))
+
+
+def dot_t(a, b):
+    return lax.dot_general(a, b, (((1,), (1,)), ((), ())), preferred_element_type=f32)
+
+
+def dot(a, b):
+    return jnp.dot(a, b, preferred_element_type=f32)
+
+
+def add_pieces(pieces, order, side, gain, w_gate, w_up, gate, up, square):
+    kv = lax.axis_index("kv")
+    pair = w_gate.shape[1] // lax.axis_size("kv")
+    for piece, s in zip(pieces, order):
+        width = piece.shape[1]
+        start = (kv ^ s) * pair
+        if width < pair:
+            start = start + side * width
+        cols = pl.ds(pl.multiple_of(start, width), width)
+        wide = piece.astype(f32)
+        scaled = (wide * gain[:, cols]).astype(bf16)
+        one = dot_t(scaled, w_gate[:, cols])
+        two = dot_t(scaled, w_up[:, cols])
+        gate = one if gate is None else gate + one
+        up = two if up is None else up + two
+        squares = jnp.sum(wide * wide, axis=1, keepdims=True)
+        square = squares if square is None else square + squares
+    return gate, up, square
+
+
+def hidden_of(gate, up, square, depth):
+    scale = lax.rsqrt(square / depth + EPSILON)
+    return (silu(gate * scale) * (up * scale)).astype(bf16)
+
+
+def copy_kernel(x, out):
+    out[...] = x[...]
+
+
+def pack_kernel(*refs):
+    *ins, out = refs
+    for s, ref in enumerate(ins):
+        out[s] = ref[...]
+
+
+def up_own_kernel(x, gain, w_gate, w_up, acc, sq):
+    n = x.shape[0]
+    gate, up, square = add_pieces(
+        [x[s] for s in range(n)], range(n), lax.axis_index("tp"), gain, w_gate, w_up, None, None, None
+    )
+    acc[0], acc[1] = gate, up
+    sq[...] = jnp.broadcast_to(square, sq.shape)
+
+
+def first_kernel(x, gain, w_gate, w_up, acc, sq, w_down, *outs):
+    n = x.shape[0]
+    gate, up, square = add_pieces(
+        [x[s] for s in range(n)], range(n), 1 - lax.axis_index("tp"), gain, w_gate, w_up,
+        acc[0], acc[1], sq[:, :1],
+    )
+    hidden = hidden_of(gate, up, square, w_gate.shape[1])
+    kv = lax.axis_index("kv")
+    for s, out in enumerate(outs):
+        width = out.shape[1]
+        cols = pl.ds(pl.multiple_of((kv ^ s) * width, width), width)
+        out[...] = dot(hidden, w_down[:, cols])
+
+
+def sum_kernel(*refs):
+    *ins, out = refs
+    total = ins[0][...]
+    for ref in ins[1:]:
+        total = total + ref[...]
+    out[...] = total
+
+
+def project_kernel(mine, other, x_own, x_other, gain, wq, wk, wz, wv, wo, middle, *rest):
+    *outs, scr = rest
+    kv = lax.axis_index("kv")
+    lower = lax.axis_index("tp") == 0
+    own, far = x_own[0].astype(f32), x_other[0].astype(f32)
+    stream = jnp.concatenate(
+        [jnp.where(lower, own, far), jnp.where(lower, far, own)], axis=1
+    )
+    mid = (stream + 0.5 * (mine[...] + other[...])).astype(bf16)
+    middle[...] = mid
+    wide = mid.astype(f32)
+    scaled = (wide * gain[...]).astype(bf16)
+    n, rows = scr.shape[:2]
+    squares = jnp.sum(wide * wide, axis=1, keepdims=True)
+    parts = [dot(scaled, w[...]) for w in (wq, wk, wz, wv, wo)]
+    parts.append(jnp.broadcast_to(squares, (wide.shape[0], LANES)))
+    at = 0
+    for part in parts:
+        for j in range(n):
+            scr[j, :, at:at + part.shape[1]] = part[j * rows:(j + 1) * rows]
+        at += part.shape[1]
+    for s, out in enumerate(outs):
+        out[...] = scr[kv ^ s]
+
+
+def state_kernel(depth, *refs):
+    *ins, old, amounts, head_gain, new, mixed = refs
+    rows, heads, keys, values = old.shape
+    nk, nv = heads * keys, heads * values
+    total = ins[0][...]
+    for ref in ins[1:]:
+        total = total + ref[...]
+    scale = lax.rsqrt(total[:, -1:] / depth + EPSILON)
+    total = total * scale
+    query = total[:, :nk] * keys ** (-0.5)
+    key = total[:, nk:2 * nk]
+    z = total[:, 2 * nk:3 * nk]
+    value = total[:, 3 * nk:3 * nk + nv]
+    out_gate = total[:, 3 * nk + nv:3 * nk + 2 * nv]
+    log_sigmoid = jnp.minimum(z, 0.0) - jnp.log1p(jnp.exp(-jnp.abs(z)))
+    decay = jnp.exp(log_sigmoid / GATE_SOFTNESS - amounts[...])
+    turned = jnp.concatenate([query, key, decay], axis=0)
+    short = -turned.shape[0] % 8
+    if short:
+        turned = jnp.concatenate([turned, jnp.zeros((short, nk), f32)], axis=0)
+    turned = turned.T
+    gated = silu(out_gate) * head_gain[...]
+    for b in range(rows):
+        for h in range(heads):
+            at = slice(h * keys, (h + 1) * keys)
+            cols = slice(h * values, (h + 1) * values)
+            q = turned[at, b:b + 1]
+            k = turned[at, rows + b:rows + b + 1]
+            d = turned[at, 2 * rows + b:2 * rows + b + 1]
+            state = d * old[b, h] + k * value[b:b + 1, cols]
+            new[b, h] = state
+            readout = jnp.sum(q * state, axis=0, keepdims=True)
+            normed = readout * lax.rsqrt(
+                jnp.mean(readout * readout, axis=1, keepdims=True) + EPSILON
+            )
+            mixed[b:b + 1, cols] = (normed * gated[b:b + 1, cols]).astype(bf16)
+
+
+def output_kernel(*refs):
+    *ins, w_out, out, scr = refs
+    kv = lax.axis_index("kv")
+    for s, ref in enumerate(ins):
+        scr[kv ^ s] = ref[...].astype(f32)
+    heads = jnp.concatenate([scr[j] for j in range(len(ins))], axis=0)
+    out[...] = dot(heads.astype(bf16), w_out[...]).astype(bf16)
+
+
+def after_kernel(middle, mine, other, after):
+    added = mine[...].astype(f32) + other[...].astype(f32)
+    after[...] = (middle[...].astype(f32) + added).astype(bf16)
+
+
+def up_block_kernel(x, gain, w_gate, w_up, acc, sq):
+    gate, up, square = add_pieces([x[...]], [0], 0, gain, w_gate, w_up, None, None, None)
+    acc[0], acc[1] = gate, up
+    sq[...] = jnp.broadcast_to(square, sq.shape)
+
+
+def second_kernel(*refs):
+    *pieces, gain, w_gate, w_up, acc, sq, w_down, mine, theirs = refs
+    gate, up, square = add_pieces(
+        [p[...] for p in pieces], range(1, len(pieces) + 1), 0, gain, w_gate, w_up,
+        acc[0], acc[1], sq[:, :1],
+    )
+    hidden = hidden_of(gate, up, square, w_gate.shape[1])
+    kv, tp = lax.axis_index("kv"), lax.axis_index("tp")
+    for out, side in ((theirs, 1 - tp), (mine, tp)):
+        width = out.shape[2]
+        for s in range(out.shape[0]):
+            cols = pl.ds(pl.multiple_of((kv ^ s) * 2 * width + side * width, width), width)
+            out[s] = dot(hidden, w_down[:, cols])
+
+
+def split_sum_kernel(mine, other, *outs):
+    for s, out in enumerate(outs):
+        out[...] = mine[s] + other[s]
+
+
+def last_kernel(after, *refs):
+    *ins, out = refs
+    total = ins[0][...]
+    for ref in ins[1:]:
+        total = total + ref[...]
+    own = out.shape[1]
+    lower = lax.axis_index("tp") == 0
+    base = jnp.where(lower, after[:, :own].astype(f32), after[:, own:].astype(f32))
+    out[...] = (base + 0.5 * total).astype(bf16)
+
+
+def body(n_kv, n_tp,
+    stream, old_state, decay_amounts, first_gain, first_gate, first_up, first_down, mixer_gain,
+    query_weight, key_weight, decay_weight, value_weight, output_gate_weight, head_gain, output_weight,
+    second_gain, second_gate, second_up, second_down,
+):
+    rows, own = stream.shape
+    pair = own * n_tp
+    depth = pair * n_kv
+    hid = first_gate.shape[1]
+    local_rows, heads, keys, values = old_state.shape
+    nk, nv = heads * keys, heads * values
+    acc_shape = [shape((2, rows, hid)), shape((rows, LANES))]
+    g1, g2, gm, gh = (g.reshape(1, -1) for g in (first_gain, second_gain, mixer_gain, head_gain))
+
+    early = call(copy_kernel, shape(stream.shape, bf16), stream, moved=16 << 20, flops=20_000_000_000)
+    pieces = [early] + send_kv([early] * (n_kv - 1), n_kv)
+    x_own = call(pack_kernel, shape((n_kv, rows, own), bf16), *pieces, flops=5_000_000_000)
+    x_other = swap(x_own, "tp", n_tp, 1)
+    wg, wu = first_gate.T, first_up.T
+    half_flops = 2 * rows * depth * hid
+    acc, sq = call(up_own_kernel, acc_shape, x_own, g1, wg, wu, flops=half_flops, limit=12)
+    blocks = call(
+        first_kernel, [shape((rows, pair))] * n_kv, x_other, g1, wg, wu, acc, sq, first_down,
+        flops=2 * half_flops, limit=16,
+    )
+    mine = call(sum_kernel, shape((rows, pair)), blocks[0], *send_kv(blocks[1:], n_kv))
+    other = swap(mine, "tp", n_tp, 1)
+    total = 3 * nk + 2 * nv + LANES
+    middle, *parts = call(
+        project_kernel, [shape((rows, pair), bf16)] + [shape((local_rows, total))] * n_kv,
+        mine, other, x_own, x_other, gm, query_weight, key_weight, decay_weight, value_weight,
+        output_gate_weight, scratch=[pltpu.VMEM((n_kv, local_rows, total), f32)],
+        flops=2 * rows * pair * total,
+    )
+    new_state, mixed = call(
+        functools.partial(state_kernel, depth),
+        [shape(old_state.shape), shape((local_rows, nv), bf16)],
+        parts[0], *send_kv(parts[1:], n_kv), old_state, decay_amounts, gh,
+        flops=8 * old_state.size,
+    )
+    product = call(
+        output_kernel, shape((rows, pair), bf16), mixed, *send_kv([mixed] * (n_kv - 1), n_kv),
+        output_weight, scratch=[pltpu.VMEM((n_kv, local_rows, nv), f32)], flops=2 * rows * nv * pair,
+    )
+    after = call(after_kernel, shape((rows, pair), bf16), middle, product, swap(product, "tp", n_tp, 1))
+    others = send_kv([after] * (n_kv - 1), n_kv)
+    wg, wu = second_gate.T, second_up.T
+    acc, sq = call(up_block_kernel, acc_shape, after, g2, wg, wu, flops=half_flops // 2, limit=12)
+    mine, theirs = call(
+        second_kernel, [shape((n_kv, rows, own))] * 2, *others, g2, wg, wu, acc, sq, second_down,
+        flops=2 * half_flops, limit=16,
+    )
+    blocks = call(split_sum_kernel, [shape((rows, own))] * n_kv, mine, swap(theirs, "tp", n_tp, 1))
+    mixed_stream = call(last_kernel, shape((rows, own), bf16), after, blocks[0], *send_kv(blocks[1:], n_kv))
+    return (mixed_stream, new_state)
 
 
 def half_block(stream, norm_gain, w_gate, w_up, w_down):
@@ -23,7 +306,7 @@
     return (stream.astype(jnp.float32) + 0.5 * summed).astype(jnp.bfloat16)
 
 
-def body(
+def wide_body(
     stream,
     old_state,
     decay_amounts,
@@ -67,7 +350,7 @@
             jnp.sum(wide_cols * wide_cols, axis=1), "kv", scatter_dimension=0, tiled=True
         ),
     )
-    row_scale = lax.rsqrt(own_squares / D + EPSILON)[:, None]
+    row_scale = lax.rsqrt(own_squares / (wide_cols.shape[1] * lax.axis_size("kv")) + EPSILON)[:, None]
     query = (query_sum * row_scale * key_dim ** (-0.5)).reshape(local_rows, local_heads, key_dim)
     keys = (key_sum * row_scale).reshape(local_rows, local_heads, key_dim)
     gate_logits = (decay_sum * row_scale).reshape(local_rows, local_heads, key_dim)
@@ -102,6 +385,9 @@
 
 
 def solution(mesh):
+    n_kv, n_tp = mesh.shape["kv"], mesh.shape["tp"]
+    few = n_kv <= 8 and n_kv & (n_kv - 1) == 0 and n_tp == 2
+    program = functools.partial(body, n_kv, n_tp) if few else wide_body
     in_specs = (
         P("dp", ("kv", "tp")),
         P(("dp", "kv"), "tp", None, None),
@@ -124,4 +410,4 @@
         P(("kv", "tp"), None),
     )
     out_specs = (P("dp", ("kv", "tp")), P(("dp", "kv"), "tp", None, None))
-    return jax.shard_map(body, mesh=mesh, in_specs=in_specs, out_specs=out_specs, check_vma=False)
+    return jax.shard_map(program, mesh=mesh, in_specs=in_specs, out_specs=out_specs, check_vma=False)

time: 172 us -> 59 us (0.34)
  blocking collectives: 60.8 us -> 0 us
  waiting for transfers between devices: 68.8 us -> 21.9 us
  starting transfers between devices: 0.12 us -> 27.8 us
  matrix products: 21.3 us -> 0 us
  between operations: 14.6 us -> 0.82 us
  Pallas kernels: 0 us -> 6.84 us
  other arithmetic: 4.73 us -> 0 us
    reduce_scatter x3 -> x0, waiting for transfers between devices: 68.8 us -> none  [the longest x2 62.4 us: half_block(): lax.psum_scatter(partial_out, ('kv', 'tp'), scatter_dimension=1, tiled=True)]
    all_gather x4 -> x0, blocking collectives: 44.1 us -> none  [the longest x2 30.4 us: half_block(): lax.all_gather(stream, ('kv', 'tp'), axis=1, tiled=True).astype(jnp.float32)]
    ppermute x0 -> x22, starting transfers between devices: none -> 27.8 us  [swap(): return lax.ppermute(x, axis, [(j, j ^ shift) for j in range(size)])]
    ppermute x0 -> x22, waiting for transfers between devices: none -> 21.9 us  [swap(): return lax.ppermute(x, axis, [(j, j ^ shift) for j in range(size)])]
    dot_general x11 -> x0, matrix products: 21.3 us -> none  [the longest x2 9.16 us: half_block(): partial_out = jnp.dot(hidden, w_down, preferred_element_type=jnp.float32)]
    unnamed x1 -> x0, blocking collectives: 16.6 us -> none
    pallas_call x0 -> x13, Pallas kernels: none -> 6.84 us  [call(): pl.pallas_call(kernel, out_shape=outs, in_specs=[vmem] * len(args), out_s...]
    convert_element_type x3 -> x0, other arithmetic: 2.67 us -> none  [the longest x2 1.99 us: half_block(): return (stream.astype(jnp.float32) + 0.5 * summed).astype(jnp.bfloat16)]
  transfers between devices with their start and end apart: 3 -> 22, of which waited for: 3 -> 17; matrix products, arithmetic and copies ran while one was open for 0% -> 0% of each run, Pallas kernels for 0% -> 2%
where the time goes in v1:
time: 59 us; the launch traced here: 58.8 us
  starting transfers between devices  27.8 us (47%)
  waiting for transfers between devices  21.9 us (37%)
  Pallas kernels  6.84 us (12%)
  local copies, waits for them, and re-layouts  1.44 us (2%)
  between operations  0.82 us (1%)
    ppermute x22, starting transfers between devices, swap(): return lax.ppermute(x, axis, [(j, j ^ shift) for j in range(size)])  27.8 us
    ppermute x22, waiting for transfers between devices, swap(): return lax.ppermute(x, axis, [(j, j ^ shift) for j in range(size)])  21.9 us
    pallas_call x13, Pallas kernels, call(): pl.pallas_call(kernel, out_shape=outs, in_specs=[vmem] * len(args), out_s...  6.84 us
    unnamed x38, local copies, waits for them, and re-layouts  1.44 us
  transfers between devices with their start and end apart: 22, of which 17 were waited for; matrix products, arithmetic and copies ran while one was open for 0% of the time, Pallas kernels for 2%

profile of v1, /device:TPU:0, one launch (start us, length us, event | category | flops | bytes accessed | tf_op | source)
XLA Modules:
  0.0 58.8 jit_solution(5499239876141919555)
XLA Ops:
  0.6 0.7 %copy-done.18 = bf16[8,256]{1,0:T(8,128)(2,1)S(1)} copy-done((bf16[8,256]{1,0:T(8,128)(2,1)S(1)}, bf16[8,256]{1,0:T(8,128)(2,1)}, u32[]{:S(2)}) %copy-start.18) | copy-done | bytes 4120
  1.3 5.1 %collective-permute-start.2 = (bf16[8,256]{1,0:T(8,128)(2,1)S(1)}, bf16[8,256]{1,0:T(8,128)(2,1)S(1)}, u32[]{:S(2)}, u32[]{:S(2)}) collective-permute-start(bf16[8,256]{1,0:T(8,128)(2,1)S(1)} %shard_map.194.refs_0_), channel_id=1, source_target_pairs={{0,6},{2,4},{4,2},{6,0},{1,7},{3,5},{5,3},{7,1},{8,14},{10,12},{12... | collective-permute-start | bytes 12296 | tf_op jit(solution)/shard_map/ppermute | solution.py:37
  6.5 0.6 %collective-permute-start = (bf16[8,256]{1,0:T(8,128)(2,1)S(1)}, bf16[8,256]{1,0:T(8,128)(2,1)S(1)}, u32[]{:S(2)}, u32[]{:S(2)}) collective-permute-start(bf16[8,256]{1,0:T(8,128)(2,1)S(1)} %shard_map.194.refs_0_), channel_id=1, source_target_pairs={{0,2},{2,0},{4,6},{6,4},{1,3},{3,1},{5,7},{7,5},{8,10},{10,8},{12,... | collective-permute-start | bytes 12296 | tf_op jit(solution)/shard_map/ppermute | solution.py:37
  7.1 0.9 %collective-permute-done.2.refs_3_ = bf16[8,256]{1,0:T(8,128)(2,1)S(1)} collective-permute-done((bf16[8,256]{1,0:T(8,128)(2,1)S(1)}, bf16[8,256]{1,0:T(8,128)(2,1)S(1)}, u32[]{:S(2)}, u32[]{:S(2)}) %collective-permute-start.2) | collective-permute-done | bytes 4128 | tf_op jit(solution)/shard_map/ppermute | solution.py:37
  8.1 2.9 %collective-permute-done.1.refs_2_ = bf16[8,256]{1,0:T(8,128)(2,1)S(1)} collective-permute-done((bf16[8,256]{1,0:T(8,128)(2,1)S(1)}, bf16[8,256]{1,0:T(8,128)(2,1)S(1)}, u32[]{:S(2)}, u32[]{:S(2)}) %collective-permute-start.1) | collective-permute-done | bytes 4128 | tf_op jit(solution)/shard_map/ppermute | solution.py:37
  11.0 0.9 %shard_map.196 = (f32[2,8,704]{2,1,0:T(8,128)S(1)}, f32[8,128]{1,0:T(8,128)S(1)}) custom-call(bf16[4,8,256]{2,1,0:T(8,128)(2,1)S(1)} %shard_map.195.x.x_own, f32[1,2048]{1,0:T(1,128)S(1)} %bitcast.16, bf16[704,2048]{1,0:T(8,128)(2,1)S(1)} %bitcast.8, bf16[704,2048]{1,0:T(8,128)(2,1)S(1)} %bitcast.10), custom_call_target="tpu_custom_call" | custom-call | flops 23068672 | bytes 5791744 | tf_op jit(solution)/shard_map/pallas_call | solution.py:25
  12.2 0.7 %copy-done.4 = bf16[704,2048]{1,0:T(8,128)(2,1)S(1)} copy-done((bf16[704,2048]{1,0:T(8,128)(2,1)S(1)}, bf16[704,2048]{1,0:T(8,128)(2,1)}, u32[]{:S(2)}) %copy-start.4) | copy-done | bytes 2883608
  12.9 1.3 %shard_map.197 = (f32[8,512]{1,0:T(8,128)S(1)}, f32[8,512]{1,0:T(8,128)S(1)}, f32[8,512]{1,0:T(8,128)S(1)}, f32[8,512]{1,0:T(8,128)S(1)}) custom-call(bf16[4,8,256]{2,1,0:T(8,128)(2,1)S(1)} %collective-permute-done.3.x.x_other, f32[1,2048]{1,0:T(1,128)S(1)} %bitcast.17, bf16[704,2048]{1,0:T(8,128)(2,1)S(1)} %bitcast.9, bf16[704,2048]{1,0:T(8,128)(2,1)S(1)} %bitcast.11, ...), custom_call_target="tpu_custom_call" | custom-call | flops 46137344 | bytes 8724480 | tf_op jit(solution)/shard_map/pallas_call | solution.py:25
  14.2 2.1 %collective-permute-start.5 = (f32[8,512]{1,0:T(8,128)S(1)}, f32[8,512]{1,0:T(8,128)S(1)}, u32[]{:S(2)}, u32[]{:S(2)}) collective-permute-start(f32[8,512]{1,0:T(8,128)S(1)} %get-tuple-element.27), channel_id=1, source_target_pairs={{0,4},{2,6},{4,0},{6,2},{1,5},{3,7},{5,1},{7,3},{8,12},{10,14},{12... | collective-permute-start | bytes 49160 | tf_op jit(solution)/shard_map/ppermute | solution.py:37
  16.3 2.3 %collective-permute-start.6 = (f32[8,512]{1,0:T(8,128)S(1)}, f32[8,512]{1,0:T(8,128)S(1)}, u32[]{:S(2)}, u32[]{:S(2)}) collective-permute-start(f32[8,512]{1,0:T(8,128)S(1)} %get-tuple-element.28), channel_id=1, source_target_pairs={{0,6},{2,4},{4,2},{6,0},{1,7},{3,5},{5,3},{7,1},{8,14},{10,12},{12... | collective-permute-start | bytes 49160 | tf_op jit(solution)/shard_map/ppermute | solution.py:37
  19.0 2.9 %collective-permute-done.6.refs_3_ = f32[8,512]{1,0:T(8,128)S(1)} collective-permute-done((f32[8,512]{1,0:T(8,128)S(1)}, f32[8,512]{1,0:T(8,128)S(1)}, u32[]{:S(2)}, u32[]{:S(2)}) %collective-permute-start.6) | collective-permute-done | bytes 16416 | tf_op jit(solution)/shard_map/ppermute | solution.py:37
  21.9 1.2 %collective-permute-done.7.other = f32[8,512]{1,0:T(8,128)S(1)} collective-permute-done((f32[8,512]{1,0:T(8,128)S(1)}, f32[8,512]{1,0:T(8,128)S(1)}, u32[]{:S(2)}, u32[]{:S(2)}) %collective-permute-start.7) | collective-permute-done | bytes 16416 | tf_op jit(solution)/shard_map/ppermute | solution.py:37
  23.7 2.7 %collective-permute-start.9 = (f32[2,1920]{1,0:T(2,128)S(1)}, f32[2,1920]{1,0:T(2,128)S(1)}, u32[]{:S(2)}, u32[]{:S(2)}) collective-permute-start(f32[2,1920]{1,0:T(2,128)S(1)} %get-tuple-element.32), channel_id=1, source_target_pairs={{0,4},{2,6},{4,0},{6,2},{1,5},{3,7},{5,1},{7,3},{8,12},{10,14},{12... | collective-permute-start | bytes 46088 | tf_op jit(solution)/shard_map/ppermute | solution.py:37
  26.4 1.5 %collective-permute-start.10 = (f32[2,1920]{1,0:T(2,128)S(1)}, f32[2,1920]{1,0:T(2,128)S(1)}, u32[]{:S(2)}, u32[]{:S(2)}) collective-permute-start(f32[2,1920]{1,0:T(2,128)S(1)} %get-tuple-element.33), channel_id=1, source_target_pairs={{0,6},{2,4},{4,2},{6,0},{1,7},{3,5},{5,3},{7,1},{8,14},{10,12},{12... | collective-permute-start | bytes 46088 | tf_op jit(solution)/shard_map/ppermute | solution.py:37
  28.3 3.6 %collective-permute-done.10.refs_3_ = f32[2,1920]{1,0:T(2,128)S(1)} collective-permute-done((f32[2,1920]{1,0:T(2,128)S(1)}, f32[2,1920]{1,0:T(2,128)S(1)}, u32[]{:S(2)}, u32[]{:S(2)}) %collective-permute-start.10) | collective-permute-done | bytes 15392 | tf_op jit(solution)/shard_map/ppermute | solution.py:37
  31.9 1.4 %shard_map.200 = (f32[2,4,64,128]{3,2,1,0:T(8,128)}, bf16[2,512]{1,0:T(2,128)(2,1)S(1)}) custom-call(f32[2,1920]{1,0:T(2,128)S(1)} %get-tuple-element.30.refs_0_, f32[2,1920]{1,0:T(2,128)S(1)} %collective-permute-done.8.refs_1_, f32[2,1920]{1,0:T(2,128)S(1)} %collective-permute-done.9.refs_2_, f32[2,1920]{1,0:T(2,128)S(1)} %collective-permute-done.10.refs_3_, ...), custom_call_target="tpu_custom_call" | custom-call | flops 524288 | bytes 327680 | tf_op jit(solution)/shard_map/pallas_call | solution.py:25
  33.3 1.5 %collective-permute-start.13 = (bf16[2,512]{1,0:T(2,128)(2,1)S(1)}, bf16[2,512]{1,0:T(2,128)(2,1)S(1)}, u32[]{:S(2)}, u32[]{:S(2)}) collective-permute-start(bf16[2,512]{1,0:T(2,128)(2,1)S(1)} %get-tuple-element.34.refs_0_), channel_id=1, source_target_pairs={{0,6},{2,4},{4,2},{6,0},{1,7},{3,5},{5,3},{7,1},{8,14},{10,12},{12... | collective-permute-start | bytes 6152 | tf_op jit(solution)/shard_map/ppermute | solution.py:37
  34.8 2.9 %collective-permute-start.11 = (bf16[2,512]{1,0:T(2,128)(2,1)S(1)}, bf16[2,512]{1,0:T(2,128)(2,1)S(1)}, u32[]{:S(2)}, u32[]{:S(2)}) collective-permute-start(bf16[2,512]{1,0:T(2,128)(2,1)S(1)} %get-tuple-element.34.refs_0_), channel_id=1, source_target_pairs={{0,2},{2,0},{4,6},{6,4},{1,3},{3,1},{5,7},{7,5},{8,10},{10,8},{12,... | collective-permute-start | bytes 6152 | tf_op jit(solution)/shard_map/ppermute | solution.py:37
  37.7 1.0 %collective-permute-done.13.refs_3_ = bf16[2,512]{1,0:T(2,128)(2,1)S(1)} collective-permute-done((bf16[2,512]{1,0:T(2,128)(2,1)S(1)}, bf16[2,512]{1,0:T(2,128)(2,1)S(1)}, u32[]{:S(2)}, u32[]{:S(2)}) %collective-permute-start.13) | collective-permute-done | bytes 2080 | tf_op jit(solution)/shard_map/ppermute | solution.py:37
  38.7 0.6 %collective-permute-done.12.refs_2_ = bf16[2,512]{1,0:T(2,128)(2,1)S(1)} collective-permute-done((bf16[2,512]{1,0:T(2,128)(2,1)S(1)}, bf16[2,512]{1,0:T(2,128)(2,1)S(1)}, u32[]{:S(2)}, u32[]{:S(2)}) %collective-permute-start.12) | collective-permute-done | bytes 2080 | tf_op jit(solution)/shard_map/ppermute | solution.py:37
  39.5 1.2 %collective-permute-done.14.other = bf16[8,512]{1,0:T(8,128)(2,1)S(1)} collective-permute-done((bf16[8,512]{1,0:T(8,128)(2,1)S(1)}, bf16[8,512]{1,0:T(8,128)(2,1)S(1)}, u32[]{:S(2)}, u32[]{:S(2)}) %collective-permute-start.14) | collective-permute-done | bytes 8224 | tf_op jit(solution)/shard_map/ppermute | solution.py:37
  40.7 2.3 %collective-permute-start.17 = (bf16[8,512]{1,0:T(8,128)(2,1)S(1)}, bf16[8,512]{1,0:T(8,128)(2,1)S(1)}, u32[]{:S(2)}, u32[]{:S(2)}) collective-permute-start(bf16[8,512]{1,0:T(8,128)(2,1)S(1)} %shard_map.202.x.after), channel_id=1, source_target_pairs={{0,6},{2,4},{4,2},{6,0},{1,7},{3,5},{5,3},{7,1},{8,14},{10,12},{12... | collective-permute-start | bytes 24584 | tf_op jit(solution)/shard_map/ppermute | solution.py:37
  43.0 1.1 %collective-permute-start.16 = (bf16[8,512]{1,0:T(8,128)(2,1)S(1)}, bf16[8,512]{1,0:T(8,128)(2,1)S(1)}, u32[]{:S(2)}, u32[]{:S(2)}) collective-permute-start(bf16[8,512]{1,0:T(8,128)(2,1)S(1)} %shard_map.202.x.after), channel_id=1, source_target_pairs={{0,4},{2,6},{4,0},{6,2},{1,5},{3,7},{5,1},{7,3},{8,12},{10,14},{12... | collective-permute-start | bytes 24584 | tf_op jit(solution)/shard_map/ppermute | solution.py:37
  44.1 1.0 %collective-permute-start.15 = (bf16[8,512]{1,0:T(8,128)(2,1)S(1)}, bf16[8,512]{1,0:T(8,128)(2,1)S(1)}, u32[]{:S(2)}, u32[]{:S(2)}) collective-permute-start(bf16[8,512]{1,0:T(8,128)(2,1)S(1)} %shard_map.202.x.after), channel_id=1, source_target_pairs={{0,2},{2,0},{4,6},{6,4},{1,3},{3,1},{5,7},{7,5},{8,10},{10,8},{12,... | collective-permute-start | bytes 24584 | tf_op jit(solution)/shard_map/ppermute | solution.py:37
  46.2 1.4 %collective-permute-done.16.refs_1_ = bf16[8,512]{1,0:T(8,128)(2,1)S(1)} collective-permute-done((bf16[8,512]{1,0:T(8,128)(2,1)S(1)}, bf16[8,512]{1,0:T(8,128)(2,1)S(1)}, u32[]{:S(2)}, u32[]{:S(2)}) %collective-permute-start.16) | collective-permute-done | bytes 8224 | tf_op jit(solution)/shard_map/ppermute | solution.py:37
  47.8 1.6 %shard_map.204 = (f32[4,8,256]{2,1,0:T(8,128)S(1)}, f32[4,8,256]{2,1,0:T(8,128)S(1)}) custom-call(bf16[8,512]{1,0:T(8,128)(2,1)S(1)} %collective-permute-done.15.refs_0_, bf16[8,512]{1,0:T(8,128)(2,1)S(1)} %collective-permute-done.16.refs_1_, bf16[8,512]{1,0:T(8,128)(2,1)S(1)} %collective-permute-done.17.refs_2_, f32[1,2048]{1,0:T(1,128)S(1)} %bitcast.19, ...), custom_call_target="tpu_custom_call" | custom-call | flops 46137344 | bytes 8732672 | tf_op jit(solution)/shard_map/pallas_call | solution.py:25
  49.4 1.2 %collective-permute-done.18.other = f32[4,8,256]{2,1,0:T(8,128)S(1)} collective-permute-done((f32[4,8,256]{2,1,0:T(8,128)S(1)}, f32[4,8,256]{2,1,0:T(8,128)S(1)}, u32[]{:S(2)}, u32[]{:S(2)}) %collective-permute-start.18) | collective-permute-done | bytes 32800 | tf_op jit(solution)/shard_map/ppermute | solution.py:37
  50.6 1.0 %collective-permute-start.19 = (f32[8,256]{1,0:T(8,128)S(1)}, f32[8,256]{1,0:T(8,128)S(1)}, u32[]{:S(2)}, u32[]{:S(2)}) collective-permute-start(f32[8,256]{1,0:T(8,128)S(1)} %get-tuple-element.40), channel_id=1, source_target_pairs={{0,2},{2,0},{4,6},{6,4},{1,3},{3,1},{5,7},{7,5},{8,10},{10,8},{12,... | collective-permute-start | bytes 24584 | tf_op jit(solution)/shard_map/ppermute | solution.py:37
  51.6 1.1 %collective-permute-start.20 = (f32[8,256]{1,0:T(8,128)S(1)}, f32[8,256]{1,0:T(8,128)S(1)}, u32[]{:S(2)}, u32[]{:S(2)}) collective-permute-start(f32[8,256]{1,0:T(8,128)S(1)} %get-tuple-element.41), channel_id=1, source_target_pairs={{0,4},{2,6},{4,0},{6,2},{1,5},{3,7},{5,1},{7,3},{8,12},{10,14},{12... | collective-permute-start | bytes 24584 | tf_op jit(solution)/shard_map/ppermute | solution.py:37
  52.7 2.3 %collective-permute-start.21 = (f32[8,256]{1,0:T(8,128)S(1)}, f32[8,256]{1,0:T(8,128)S(1)}, u32[]{:S(2)}, u32[]{:S(2)}) collective-permute-start(f32[8,256]{1,0:T(8,128)S(1)} %get-tuple-element.42), channel_id=1, source_target_pairs={{0,6},{2,4},{4,2},{6,0},{1,7},{3,5},{5,3},{7,1},{8,14},{10,12},{12... | collective-permute-start | bytes 24584 | tf_op jit(solution)/shard_map/ppermute | solution.py:37
  55.0 1.2 %collective-permute-done.20.refs_2_ = f32[8,256]{1,0:T(8,128)S(1)} collective-permute-done((f32[8,256]{1,0:T(8,128)S(1)}, f32[8,256]{1,0:T(8,128)S(1)}, u32[]{:S(2)}, u32[]{:S(2)}) %collective-permute-start.20) | collective-permute-done | bytes 8224 | tf_op jit(solution)/shard_map/ppermute | solution.py:37
  56.2 2.0 %collective-permute-done.21.refs_3_ = f32[8,256]{1,0:T(8,128)S(1)} collective-permute-done((f32[8,256]{1,0:T(8,128)S(1)}, f32[8,256]{1,0:T(8,128)S(1)}, u32[]{:S(2)}, u32[]{:S(2)}) %collective-permute-start.21) | collective-permute-done | bytes 8224 | tf_op jit(solution)/shard_map/ppermute | solution.py:37
  (63 shorter events, 3.8 us)
Async XLA Ops:
  1.3 6.7 %collective-permute-start.2 = (bf16[8,256]{1,0:T(8,128)(2,1)S(1)}, bf16[8,256]{1,0:T(8,128)(2,1)S(1)}, u32[]{:S(2)}, u32[]{:S(2)}) collective-permute-start(bf16[8,256]{1,0:T(8,128)(2,1)S(1)} %shard_map.194.refs_0_), channel_id=1, source_target_pairs={{0,6},{2,4},{4,2},{6,0},{1,7},{3,5},{5,3},{7,1},{8,14},{10,12},{12... | collective-permute-start | bytes 12296 | tf_op jit(solution)/shard_map/ppermute | solution.py:37
  6.5 4.5 %collective-permute-start.1 = (bf16[8,256]{1,0:T(8,128)(2,1)S(1)}, bf16[8,256]{1,0:T(8,128)(2,1)S(1)}, u32[]{:S(2)}, u32[]{:S(2)}) collective-permute-start(bf16[8,256]{1,0:T(8,128)(2,1)S(1)} %shard_map.194.refs_0_), channel_id=1, source_target_pairs={{0,4},{2,6},{4,0},{6,2},{1,5},{3,7},{5,1},{7,3},{8,12},{10,14},{12... | collective-permute-start | bytes 12296 | tf_op jit(solution)/shard_map/ppermute | solution.py:37
  6.5 4.5 %collective-permute-start = (bf16[8,256]{1,0:T(8,128)(2,1)S(1)}, bf16[8,256]{1,0:T(8,128)(2,1)S(1)}, u32[]{:S(2)}, u32[]{:S(2)}) collective-permute-start(bf16[8,256]{1,0:T(8,128)(2,1)S(1)} %shard_map.194.refs_0_), channel_id=1, source_target_pairs={{0,2},{2,0},{4,6},{6,4},{1,3},{3,1},{5,7},{7,5},{8,10},{10,8},{12,... | collective-permute-start | bytes 12296 | tf_op jit(solution)/shard_map/ppermute | solution.py:37
  11.0 1.2 %collective-permute-start.3 = (bf16[4,8,256]{2,1,0:T(8,128)(2,1)S(1)}, bf16[4,8,256]{2,1,0:T(8,128)(2,1)S(1)}, u32[]{:S(2)}, u32[]{:S(2)}) collective-permute-start(bf16[4,8,256]{2,1,0:T(8,128)(2,1)S(1)} %shard_map.195.x.x_own), channel_id=1, source_target_pairs={{0,1},{1,0},{2,3},{3,2},{4,5},{5,4},{6,7},{7,6},{8,9},{9,8},{10,11... | collective-permute-start | bytes 49160 | tf_op jit(solution)/shard_map/ppermute | solution.py:37
  12.8 10.2 %copy-start.11 = (bf16[512,256]{1,0:T(8,128)(2,1)S(1)}, bf16[512,256]{1,0:T(8,128)(2,1)}, u32[]{:S(2)}) copy-start(bf16[512,256]{1,0:T(8,128)(2,1)} %wk.1) | copy-start | bytes 786436
  12.9 10.2 %copy-start.12 = (bf16[512,256]{1,0:T(8,128)(2,1)S(1)}, bf16[512,256]{1,0:T(8,128)(2,1)}, u32[]{:S(2)}) copy-start(bf16[512,256]{1,0:T(8,128)(2,1)} %wz.1) | copy-start | bytes 786436
  12.9 10.2 %copy-start.15 = (f32[512]{0:T(512)S(1)}, f32[512]{0:T(512)}, u32[]{:S(2)}) copy-start(f32[512]{0:T(512)} %param.26) | copy-start | bytes 6148
  12.9 19.0 %copy-start.9 = (f32[2,4,64,128]{3,2,1,0:T(8,128)S(1)}, f32[2,4,64,128]{3,2,1,0:T(8,128)}, u32[]{:S(2)}) copy-start(f32[2,4,64,128]{3,2,1,0:T(8,128)} %refs_4_.2) | copy-start | bytes 786436
  12.9 19.0 %copy-start.16 = (f32[2,256]{1,0:T(2,128)S(1)}, f32[2,256]{1,0:T(2,128)}, u32[]{:S(2)}) copy-start(f32[2,256]{1,0:T(2,128)} %refs_5_.1) | copy-start | bytes 6148
  12.9 19.0 %copy-start.17 = (f32[512]{0:T(512)S(1)}, f32[512]{0:T(512)}, u32[]{:S(2)}) copy-start(f32[512]{0:T(512)} %param.32) | copy-start | bytes 6148
  12.9 26.4 %copy-start.8 = (bf16[512,512]{1,0:T(8,128)(2,1)S(1)}, bf16[512,512]{1,0:T(8,128)(2,1)}, u32[]{:S(2)}) copy-start(bf16[512,512]{1,0:T(8,128)(2,1)} %refs_4_.3) | copy-start | bytes 1572868
  12.9 32.2 %copy-start.3 = (bf16[2048,704]{0,1:T(8,128)(2,1)S(1)}, bf16[2048,704]{0,1:T(8,128)(2,1)}, u32[]{:S(2)}) copy-start(bf16[2048,704]{0,1:T(8,128)(2,1)} %param.36) | copy-start | bytes 8650756
  14.2 30.9 %copy-start.2 = (bf16[2048,704]{0,1:T(8,128)(2,1)S(1)}, bf16[2048,704]{0,1:T(8,128)(2,1)}, u32[]{:S(2)}) copy-start(bf16[2048,704]{0,1:T(8,128)(2,1)} %param.35) | copy-start | bytes 8650756
  14.2 30.9 %copy-start.14 = (f32[2048]{0:T(1024)S(1)}, f32[2048]{0:T(1024)}, u32[]{:S(2)}) copy-start(f32[2048]{0:T(1024)} %param.34) | copy-start | bytes 24580
  14.2 4.4 %collective-permute-start.4 = (f32[8,512]{1,0:T(8,128)S(1)}, f32[8,512]{1,0:T(8,128)S(1)}, u32[]{:S(2)}, u32[]{:S(2)}) collective-permute-start(f32[8,512]{1,0:T(8,128)S(1)} %get-tuple-element.26), channel_id=1, source_target_pairs={{0,2},{2,0},{4,6},{6,4},{1,3},{3,1},{5,7},{7,5},{8,10},{10,8},{12,... | collective-permute-start | bytes 49160 | tf_op jit(solution)/shard_map/ppermute | solution.py:37
  14.2 4.7 %collective-permute-start.5 = (f32[8,512]{1,0:T(8,128)S(1)}, f32[8,512]{1,0:T(8,128)S(1)}, u32[]{:S(2)}, u32[]{:S(2)}) collective-permute-start(f32[8,512]{1,0:T(8,128)S(1)} %get-tuple-element.27), channel_id=1, source_target_pairs={{0,4},{2,6},{4,0},{6,2},{1,5},{3,7},{5,1},{7,3},{8,12},{10,14},{12... | collective-permute-start | bytes 49160 | tf_op jit(solution)/shard_map/ppermute | solution.py:37
  16.3 5.5 %collective-permute-start.6 = (f32[8,512]{1,0:T(8,128)S(1)}, f32[8,512]{1,0:T(8,128)S(1)}, u32[]{:S(2)}, u32[]{:S(2)}) collective-permute-start(f32[8,512]{1,0:T(8,128)S(1)} %get-tuple-element.28), channel_id=1, source_target_pairs={{0,6},{2,4},{4,2},{6,0},{1,7},{3,5},{5,3},{7,1},{8,14},{10,12},{12... | collective-permute-start | bytes 49160 | tf_op jit(solution)/shard_map/ppermute | solution.py:37
  21.9 1.2 %collective-permute-start.7 = (f32[8,512]{1,0:T(8,128)S(1)}, f32[8,512]{1,0:T(8,128)S(1)}, u32[]{:S(2)}, u32[]{:S(2)}) collective-permute-start(f32[8,512]{1,0:T(8,128)S(1)} %shard_map.198.mine), channel_id=1, source_target_pairs={{0,1},{1,0},{2,3},{3,2},{4,5},{5,4},{6,7},{7,6},{8,9},{9,8},{10,11... | collective-permute-start | bytes 49160 | tf_op jit(solution)/shard_map/ppermute | solution.py:37
  23.5 4.4 %collective-permute-start.8 = (f32[2,1920]{1,0:T(2,128)S(1)}, f32[2,1920]{1,0:T(2,128)S(1)}, u32[]{:S(2)}, u32[]{:S(2)}) collective-permute-start(f32[2,1920]{1,0:T(2,128)S(1)} %get-tuple-element.31), channel_id=1, source_target_pairs={{0,2},{2,0},{4,6},{6,4},{1,3},{3,1},{5,7},{7,5},{8,10},{10,8},{12,... | collective-permute-start | bytes 46088 | tf_op jit(solution)/shard_map/ppermute | solution.py:37
  23.7 4.6 %collective-permute-start.9 = (f32[2,1920]{1,0:T(2,128)S(1)}, f32[2,1920]{1,0:T(2,128)S(1)}, u32[]{:S(2)}, u32[]{:S(2)}) collective-permute-start(f32[2,1920]{1,0:T(2,128)S(1)} %get-tuple-element.32), channel_id=1, source_target_pairs={{0,4},{2,6},{4,0},{6,2},{1,5},{3,7},{5,1},{7,3},{8,12},{10,14},{12... | collective-permute-start | bytes 46088 | tf_op jit(solution)/shard_map/ppermute | solution.py:37
  26.4 5.5 %collective-permute-start.10 = (f32[2,1920]{1,0:T(2,128)S(1)}, f32[2,1920]{1,0:T(2,128)S(1)}, u32[]{:S(2)}, u32[]{:S(2)}) collective-permute-start(f32[2,1920]{1,0:T(2,128)S(1)} %get-tuple-element.33), channel_id=1, source_target_pairs={{0,6},{2,4},{4,2},{6,0},{1,7},{3,5},{5,3},{7,1},{8,14},{10,12},{12... | collective-permute-start | bytes 46088 | tf_op jit(solution)/shard_map/ppermute | solution.py:37
  33.3 5.4 %collective-permute-start.13 = (bf16[2,512]{1,0:T(2,128)(2,1)S(1)}, bf16[2,512]{1,0:T(2,128)(2,1)S(1)}, u32[]{:S(2)}, u32[]{:S(2)}) collective-permute-start(bf16[2,512]{1,0:T(2,128)(2,1)S(1)} %get-tuple-element.34.refs_0_), channel_id=1, source_target_pairs={{0,6},{2,4},{4,2},{6,0},{1,7},{3,5},{5,3},{7,1},{8,14},{10,12},{12... | collective-permute-start | bytes 6152 | tf_op jit(solution)/shard_map/ppermute | solution.py:37
  34.8 4.5 %collective-permute-start.12 = (bf16[2,512]{1,0:T(2,128)(2,1)S(1)}, bf16[2,512]{1,0:T(2,128)(2,1)S(1)}, u32[]{:S(2)}, u32[]{:S(2)}) collective-permute-start(bf16[2,512]{1,0:T(2,128)(2,1)S(1)} %get-tuple-element.34.refs_0_), channel_id=1, source_target_pairs={{0,4},{2,6},{4,0},{6,2},{1,5},{3,7},{5,1},{7,3},{8,12},{10,14},{12... | collective-permute-start | bytes 6152 | tf_op jit(solution)/shard_map/ppermute | solution.py:37
  34.8 4.5 %collective-permute-start.11 = (bf16[2,512]{1,0:T(2,128)(2,1)S(1)}, bf16[2,512]{1,0:T(2,128)(2,1)S(1)}, u32[]{:S(2)}, u32[]{:S(2)}) collective-permute-start(bf16[2,512]{1,0:T(2,128)(2,1)S(1)} %get-tuple-element.34.refs_0_), channel_id=1, source_target_pairs={{0,2},{2,0},{4,6},{6,4},{1,3},{3,1},{5,7},{7,5},{8,10},{10,8},{12,... | collective-permute-start | bytes 6152 | tf_op jit(solution)/shard_map/ppermute | solution.py:37
  39.5 1.2 %collective-permute-start.14 = (bf16[8,512]{1,0:T(8,128)(2,1)S(1)}, bf16[8,512]{1,0:T(8,128)(2,1)S(1)}, u32[]{:S(2)}, u32[]{:S(2)}) collective-permute-start(bf16[8,512]{1,0:T(8,128)(2,1)S(1)} %shard_map.201.mine), channel_id=1, source_target_pairs={{0,1},{1,0},{2,3},{3,2},{4,5},{5,4},{6,7},{7,6},{8,9},{9,8},{10,11... | collective-permute-start | bytes 24584 | tf_op jit(solution)/shard_map/ppermute | solution.py:37
  40.7 5.5 %collective-permute-start.17 = (bf16[8,512]{1,0:T(8,128)(2,1)S(1)}, bf16[8,512]{1,0:T(8,128)(2,1)S(1)}, u32[]{:S(2)}, u32[]{:S(2)}) collective-permute-start(bf16[8,512]{1,0:T(8,128)(2,1)S(1)} %shard_map.202.x.after), channel_id=1, source_target_pairs={{0,6},{2,4},{4,2},{6,0},{1,7},{3,5},{5,3},{7,1},{8,14},{10,12},{12... | collective-permute-start | bytes 24584 | tf_op jit(solution)/shard_map/ppermute | solution.py:37
  43.0 4.5 %collective-permute-start.16 = (bf16[8,512]{1,0:T(8,128)(2,1)S(1)}, bf16[8,512]{1,0:T(8,128)(2,1)S(1)}, u32[]{:S(2)}, u32[]{:S(2)}) collective-permute-start(bf16[8,512]{1,0:T(8,128)(2,1)S(1)} %shard_map.202.x.after), channel_id=1, source_target_pairs={{0,4},{2,6},{4,0},{6,2},{1,5},{3,7},{5,1},{7,3},{8,12},{10,14},{12... | collective-permute-start | bytes 24584 | tf_op jit(solution)/shard_map/ppermute | solution.py:37
  44.1 3.7 %collective-permute-start.15 = (bf16[8,512]{1,0:T(8,128)(2,1)S(1)}, bf16[8,512]{1,0:T(8,128)(2,1)S(1)}, u32[]{:S(2)}, u32[]{:S(2)}) collective-permute-start(bf16[8,512]{1,0:T(8,128)(2,1)S(1)} %shard_map.202.x.after), channel_id=1, source_target_pairs={{0,2},{2,0},{4,6},{6,4},{1,3},{3,1},{5,7},{7,5},{8,10},{10,8},{12,... | collective-permute-start | bytes 24584 | tf_op jit(solution)/shard_map/ppermute | solution.py:37
  49.4 1.2 %collective-permute-start.18 = (f32[4,8,256]{2,1,0:T(8,128)S(1)}, f32[4,8,256]{2,1,0:T(8,128)S(1)}, u32[]{:S(2)}, u32[]{:S(2)}) collective-permute-start(f32[4,8,256]{2,1,0:T(8,128)S(1)} %get-tuple-element.38), channel_id=1, source_target_pairs={{0,1},{1,0},{2,3},{3,2},{4,5},{5,4},{6,7},{7,6},{8,9},{9,8},{10,11... | collective-permute-start | bytes 98312 | tf_op jit(solution)/shard_map/ppermute | solution.py:37
  50.6 4.4 %collective-permute-start.19 = (f32[8,256]{1,0:T(8,128)S(1)}, f32[8,256]{1,0:T(8,128)S(1)}, u32[]{:S(2)}, u32[]{:S(2)}) collective-permute-start(f32[8,256]{1,0:T(8,128)S(1)} %get-tuple-element.40), channel_id=1, source_target_pairs={{0,2},{2,0},{4,6},{6,4},{1,3},{3,1},{5,7},{7,5},{8,10},{10,8},{12,... | collective-permute-start | bytes 24584 | tf_op jit(solution)/shard_map/ppermute | solution.py:37
  51.6 4.6 %collective-permute-start.20 = (f32[8,256]{1,0:T(8,128)S(1)}, f32[8,256]{1,0:T(8,128)S(1)}, u32[]{:S(2)}, u32[]{:S(2)}) collective-permute-start(f32[8,256]{1,0:T(8,128)S(1)} %get-tuple-element.41), channel_id=1, source_target_pairs={{0,4},{2,6},{4,0},{6,2},{1,5},{3,7},{5,1},{7,3},{8,12},{10,14},{12... | collective-permute-start | bytes 24584 | tf_op jit(solution)/shard_map/ppermute | solution.py:37
  52.7 5.4 %collective-permute-start.21 = (f32[8,256]{1,0:T(8,128)S(1)}, f32[8,256]{1,0:T(8,128)S(1)}, u32[]{:S(2)}, u32[]{:S(2)}) collective-permute-start(f32[8,256]{1,0:T(8,128)S(1)} %get-tuple-element.42), channel_id=1, source_target_pairs={{0,6},{2,4},{4,2},{6,0},{1,7},{3,5},{5,3},{7,1},{8,14},{10,12},{12... | collective-permute-start | bytes 24584 | tf_op jit(solution)/shard_map/ppermute | solution.py:37
  (9 other events, 64.9 us)
